TPU v7x, 32 devices: a whole 2x2x4 slice. The times are simulated.
32 devices in a mesh: sp: 4 (over z), fs: 4 (over y, x), tp: 2 (over core).
Axes of the slice: x: 2, y: 2, z: 4, core: 2. Of those that a mesh axis runs over, the one named last changes fastest.
Arguments:
- tokens: bfloat16 [4096, 2048], P(('fs', 'sp')), parts along dimension 0, may hold values from -6 to 6
- norm_gain: float32 [2048], replicated, may hold values from 0.1 to 1.9
- w_query: bfloat16 [2048, 1024], P('sp', 'tp'), may hold values from -0.080939698 to 0.080939698
- w_key: bfloat16 [2048, 256], P('sp', 'tp'), may hold values from -0.080939698 to 0.080939698
- w_value: bfloat16 [2048, 256], P('sp', 'tp'), may hold values from -0.125 to 0.125
- w_conv_in: bfloat16 [2048, 1024], P('sp', 'tp'), may hold values from -0.125 to 0.125
- w_conv_gate: bfloat16 [2048, 1024], P('sp', 'tp'), may hold values from -0.125 to 0.125
- sink_logit: float32 [16], P('tp'), may hold values from 2 to 6
- conv_taps: float32 [31, 1024], P(None, 'tp'), may hold values from -5.3881591 to 5.3881591
- conv_bias: float32 [1024], P('tp'), may hold values from -0.9 to 5.9
- channel_gain: float32 [1024], P('tp'), may hold values from 0.1 to 1.9
- channel_shift: float32 [1024], P('tp'), may hold values from -3 to 3
- w_attn_out: bfloat16 [1024, 2048], P(None, 'sp'), may hold values from -1.5 to 1.5
- w_conv_out: bfloat16 [1024, 2048], P(None, 'sp'), may hold values from -0.1875 to 0.1875
Outputs:
- output: bfloat16 [4096, 2048], P(('fs', 'sp', 'tp')), parts along dimension 0
There are 4 independent parts, one for each index of `fs`. A program takes and returns all parts, laid end to end along the dimension named above; an argument that names none is the same for every part. Nothing has to cross between parts.
All inputs are finite; a program needn't handle non-finite values.
Results may differ from a plain program's by a relative error of at most 0.011.
Values may be sent and summed in bfloat16 or wider, within the bound.
No kernel may reach another device: no remote copies, remote signals or barrier semaphores. Data moves between devices by JAX's collectives and lax.ppermute only.
A program may use at most 64 MiB of HBM per device.

v0:
```python
import jax
import jax.numpy as jnp
from jax import lax
from jax.sharding import PartitionSpec as P

HEAD_DIM = 64
WINDOW = 128
GRID_W = 64


EPSILON = 1e-06
NEGATIVE = -1e30
ROPE_BASE = 10000.0


def padded(block, sides, width):
    for axis, dim in sides:
        count = lax.axis_size(axis)
        forward = [(i, i + 1) for i in range(count - 1)]
        backward = [(target, source) for source, target in forward]
        low = lax.ppermute(
            lax.slice_in_dim(block, block.shape[dim] - width, None, axis=dim), axis, forward
        )
        high = lax.ppermute(lax.slice_in_dim(block, 0, width, axis=dim), axis, backward)
        block = jnp.concatenate([low, block, high], axis=dim)
    return block


def rotate_pairs(values, positions):
    middle = values.shape[-1] // 2
    inverse = ROPE_BASE ** (-jnp.arange(middle, dtype=jnp.float32) / middle)
    angles = positions.astype(jnp.float32)[:, None] * inverse[None, :]
    cosine = jnp.cos(angles)[:, None, :]
    sine_table = jnp.sin(angles)[:, None, :]
    leading = values[..., :middle]
    trailing = values[..., middle:]
    return jnp.concatenate(
        [leading * cosine - trailing * sine_table, leading * sine_table + trailing * cosine],
        axis=-1,
    )


def grid_rotate(values, positions):
    middle = values.shape[-1] // 2
    return jnp.concatenate(
        [
            rotate_pairs(values[..., :middle], positions // GRID_W),
            rotate_pairs(values[..., middle:], positions % GRID_W),
        ],
        axis=-1,
    )


def local(
    tokens,
    norm_gain,
    w_query,
    w_key,
    w_value,
    w_conv_in,
    w_conv_gate,
    sink_logit,
    conv_taps,
    conv_bias,
    channel_gain,
    channel_shift,
    w_attn_out,
    w_conv_out,
):
    rows_here = tokens.shape[0]
    offset = lax.axis_index("sp") * rows_here
    total = rows_here * lax.axis_size("sp")
    tp_count = lax.axis_size("tp")
    token_float = tokens.astype(jnp.float32)
    normed = (
        token_float
        * lax.rsqrt(jnp.mean(token_float * token_float, axis=-1, keepdims=True) + EPSILON)
        * norm_gain[None, :]
    ).astype(jnp.bfloat16)
    head_cols = w_query.shape[1]
    kv_cols = w_key.shape[1]
    chan_cols = w_conv_in.shape[1]
    piece_query = lax.all_gather(w_query, "sp", axis=0, tiled=True)
    piece_key = lax.all_gather(w_key, "sp", axis=0, tiled=True)
    piece_value = lax.all_gather(w_value, "sp", axis=0, tiled=True)
    piece_conv = lax.all_gather(w_conv_in, "sp", axis=0, tiled=True)
    piece_gate = lax.all_gather(w_conv_gate, "sp", axis=0, tiled=True)
    query_acc = jnp.dot(normed, piece_query, preferred_element_type=jnp.float32)
    pair_acc = jnp.dot(
        normed,
        jnp.concatenate([piece_key, piece_value], axis=1),
        preferred_element_type=jnp.float32,
    )
    conv_acc = jnp.dot(
        normed,
        jnp.concatenate([piece_conv, piece_gate], axis=1),
        preferred_element_type=jnp.float32,
    )
    positions = offset + jnp.arange(rows_here, dtype=jnp.int32)
    heads_here = head_cols // HEAD_DIM
    kv_here = kv_cols // HEAD_DIM
    group = heads_here // kv_here
    query = grid_rotate(query_acc.reshape(rows_here, heads_here, HEAD_DIM), positions).astype(
        jnp.bfloat16
    )
    keys = grid_rotate(pair_acc[:, :kv_cols].reshape(rows_here, kv_here, HEAD_DIM), positions)
    keys = keys.astype(jnp.bfloat16).reshape(rows_here, kv_cols)
    values = pair_acc[:, kv_cols:].astype(jnp.bfloat16)
    stacked = jnp.concatenate([keys, values], axis=1)
    extended = padded(stacked, (("sp", 0),), WINDOW)
    block = min(rows_here, 512)
    span = block + 2 * WINDOW
    sinks = sink_logit.reshape(kv_here, group)[:, :, None, None]
    queries = query.reshape(block, kv_here, group, HEAD_DIM)
    near_keys = extended[:, :kv_cols].reshape(span, kv_here, HEAD_DIM)
    near_values = extended[:, kv_cols:].reshape(span, kv_here, HEAD_DIM)
    scores = jnp.einsum(
        "qkgd,skd->kgqs", queries, near_keys, preferred_element_type=jnp.float32
    ) * HEAD_DIM ** (-0.5)
    query_pos = offset + 0 + jnp.arange(block, dtype=jnp.int32)
    key_pos = offset + 0 - WINDOW + jnp.arange(span, dtype=jnp.int32)
    valid = (
        (jnp.abs(query_pos[:, None] - key_pos[None, :]) <= WINDOW)
        & (key_pos[None, :] >= 0)
        & (key_pos[None, :] < total)
    )
    scores = jnp.where(valid[None, None], scores, NEGATIVE)
    top = jnp.maximum(jnp.max(scores, axis=-1, keepdims=True), sinks)
    raised = jnp.exp(scores - top)
    denominator = jnp.sum(raised, axis=-1, keepdims=True) + jnp.exp(sinks - top)
    probs = (raised / denominator).astype(jnp.bfloat16)
    mixed = jnp.einsum("kgqs,skd->qkgd", probs, near_values, preferred_element_type=jnp.float32)
    outputs = mixed.astype(jnp.bfloat16).reshape(block, head_cols)
    glu = (conv_acc[:, :chan_cols] * jax.nn.sigmoid(conv_acc[:, chan_cols:])).astype(jnp.bfloat16)
    reach = conv_taps.shape[0] // 2
    rims = padded(glu, (("sp", 0),), reach)
    filtered = jnp.zeros((rows_here, chan_cols), jnp.float32) + conv_bias[None, :]
    for shift_index in range(conv_taps.shape[0]):
        filtered = filtered + conv_taps[shift_index][None, :] * rims[
            shift_index : shift_index + rows_here
        ].astype(jnp.float32)
    channel_total = chan_cols * tp_count
    centre = lax.psum(jnp.sum(filtered, axis=-1), "tp")[:, None] / channel_total
    centred = filtered - centre
    spread = lax.psum(jnp.sum(centred * centred, axis=-1), "tp")[:, None] / channel_total
    conv_out = jax.nn.silu(
        centred * lax.rsqrt(spread + EPSILON) * channel_gain[None, :] + channel_shift[None, :]
    ).astype(jnp.bfloat16)
    features = jnp.concatenate([outputs, conv_out], axis=1)
    tp_here = lax.axis_index("tp")
    own_rows = jnp.concatenate(
        [
            lax.dynamic_slice_in_dim(w_attn_out, tp_here * head_cols, head_cols, 0),
            lax.dynamic_slice_in_dim(w_conv_out, tp_here * chan_cols, chan_cols, 0),
        ],
        axis=0,
    )
    own_whole = lax.all_gather(own_rows, "sp", axis=1, tiled=True)
    result = lax.psum_scatter(
        jnp.dot(features, own_whole, preferred_element_type=jnp.float32).astype(jnp.bfloat16),
        "tp",
        scatter_dimension=0,
        tiled=True,
    )
    return result


def solution(mesh):
    in_specs = (
        P(("fs", "sp"), None),
        P(),
        P("sp", "tp"),
        P("sp", "tp"),
        P("sp", "tp"),
        P("sp", "tp"),
        P("sp", "tp"),
        P("tp"),
        P(None, "tp"),
        P("tp"),
        P("tp"),
        P("tp"),
        P(None, "sp"),
        P(None, "sp"),
    )
    out_specs = P(("fs", "sp", "tp"), None)
    return jax.shard_map(local, mesh=mesh, in_specs=in_specs, out_specs=out_specs, check_vma=False)
```

profile of v0, /device:TPU:0, one launch (start us, length us, event | category | flops | bytes accessed | tf_op | source)
XLA Modules:
  0.0 263.5 jit_solution(13735289390232705822)
XLA Ops:
  6.5 0.7 all-gather.7.cloned.1.call-update
  7.3 0.0 all-gather.9.cloned.1.call-start
  7.3 0.7 all-gather.9.cloned.1.call-update
  8.0 0.0 all-gather.5.cloned.1.call-start
  8.1 0.7 all-gather.5.cloned.1.call-update
  8.8 0.0 all-gather.11.cloned.1.call-start
  8.8 1.3 constant_dynamic-slice_fusion
  10.1 1.0 pad_maximum_fusion
  11.1 0.0 all-gather.11.cloned.1.call-update
  11.2 0.0 reduce-scatter.2.cloned.1.call-start
  11.3 0.3 fusion.6
  11.6 23.1 %all_gather.18 = bf16[2048,128]{1,0:T(8,128)(2,1)S(1)} all-gather(bf16[512,128]{1,0:T(8,128)(2,1)S(1)} %copy-done.1), channel_id=1, replica_groups=mesh['sp'=4,'fs'=4,'tp'=2] {'sp'}, dimensions={0}, use_global_device_ids=true | all-gather | bytes 655360 | tf_op jit(solution)/shard_map/all_gather | solution.py:84
  34.7 21.7 %all_gather.19 = bf16[2048,128]{1,0:T(8,128)(2,1)S(1)} all-gather(bf16[512,128]{1,0:T(8,128)(2,1)S(1)} %copy-done.2), channel_id=1, replica_groups=mesh['sp'=4,'fs'=4,'tp'=2] {'sp'}, dimensions={0}, use_global_device_ids=true | all-gather | bytes 655360 | tf_op jit(solution)/shard_map/all_gather | solution.py:85
  56.4 0.7 fusion.11
  57.1 0.2 multiply_cosine_fusion.1
  57.4 1.5 collective-permute-start
  58.9 1.3 collective-permute-start.1
  60.3 0.3 fusion.24
  60.6 0.1 max.18
  60.7 1.5 collective-permute-done
  62.2 7.0 %collective-permute-done.1 = bf16[128,256]{0,1:T(8,128)(2,1)S(1)} collective-permute-done((bf16[128,256]{0,1:T(8,128)(2,1)S(1)}, bf16[128,256]{0,1:T(8,128)(2,1)S(1)}, u32[]{:S(2)}, u32[]{:S(2)}) %collective-permute-start.1) | collective-permute-done | bytes 65568 | tf_op jit(solution)/shard_map/ppermute | solution.py:24
  69.2 1.9 all-gather.7.cloned.1.call-done
  71.1 47.3 %all-gather.9.cloned.1.call-done = bf16[2048,512]{1,0:T(8,128)(2,1)} async-done(((bf16[512,512]{1,0:T(8,128)(2,1)}), bf16[2048,512]{1,0:T(8,128)(2,1)}) %all-gather.9.cloned.1.call-update) | async-done | bytes 2097168 | tf_op jit(solution)/shard_map/all_gather | solution.py:87
  118.4 3.5 %fusion = f32[256,1024]{1,0:T(8,128)S(1)} fusion(bf16[2048,512]{1,0:T(8,128)(2,1)} %all-gather.9.cloned.1.call-done, bf16[2048,512]{1,0:T(8,128)(2,1)} %all-gather.7.cloned.1.call-done, bf16[256,2048]{1,0:T(8,128)(2,1)S(1)} %copy-done, f32[2048]{0:T(1024)S(1)} %copy-done.7, f32[256]{0:T(256)S(1)} %add_rsqrt_fusion.1), kind=kOutput, calls=%fused_computation | convolution fusion | flops 1084227584 | bytes 6300672 | tf_op jit(solution)/shard_map/dot_general | solution.py:94
  121.9 0.1 fusion.22
  122.1 2.1 collective-permute-start.2
  124.2 1.3 collective-permute-start.3
  125.5 39.2 %all-gather.5.cloned.1.call-done = bf16[2048,512]{1,0:T(8,128)(2,1)} async-done(((bf16[512,512]{1,0:T(8,128)(2,1)}), bf16[2048,512]{1,0:T(8,128)(2,1)}) %all-gather.5.cloned.1.call-update) | async-done | bytes 2097168 | tf_op jit(solution)/shard_map/all_gather | solution.py:83
  164.6 2.6 fusion.74
  167.2 0.1 subtract_convert_fusion.1
  167.3 0.8 fusion.5
  168.2 0.1 broadcast_maximum_fusion
  168.2 0.9 fusion.4
  169.1 0.1 exponential_add_fusion
  169.2 0.0 copy-start.4
  169.2 0.0 copy-start.5
  169.2 0.0 copy-start.6
  169.3 1.2 fusion.10
  170.5 0.1 copy.27
  170.7 3.1 %fusion.77 = (f32[256]{0:T(256)S(1)}, f32[256,512]{1,0:T(8,128)S(1)}) fusion(bf16[15,512]{1,0:T(8,128)(2,1)S(1)} %collective-permute-done.3, bf16[256,512]{1,0:T(8,128)(2,1)S(1)} %fusion.22, f32[512]{0:T(512)S(1)} %bitcast.106, f32[512]{0:T(512)S(1)} %bitcast.107, f32[512]{0:T(512)S(1)} %bitcast.78, f32[512]{0:T(512)S(1)} %bitcast.79, f32[512]{0:T(512)S(1)} %bitcast.80, ...), kind=kLoop, calls=%fused_computation.167 | loop fusion | flops 24116992 | bytes 883712 | tf_op jit(solution)/shard_map/reduce_sum | solution.py:143
  173.8 2.5 psum.14
  176.2 0.2 multiply_reduce_fusion
  176.4 2.5 psum.15
  178.9 0.3 multiply_convert_fusion
  179.2 66.3 %all-gather.11.cloned.1.call-done = bf16[1024,2048]{1,0:T(8,128)(2,1)} async-done(((bf16[1024,512]{1,0:T(8,128)(2,1)}), bf16[1024,2048]{1,0:T(8,128)(2,1)}) %all-gather.11.cloned.1.call-update) | async-done | bytes 4194320 | tf_op jit(solution)/shard_map/all_gather | solution.py:158
  245.5 4.5 %convolution_convert_fusion = bf16[256,2048]{1,0:T(8,128)(2,1)} fusion(bf16[1024,2048]{1,0:T(8,128)(2,1)} %all-gather.11.cloned.1.call-done, bf16[256,512]{1,0:T(8,128)(2,1)S(1)} %multiply_convert_fusion, bf16[256,512]{1,0:T(8,128)(2,1)S(1)} %copy.27), kind=kOutput, calls=%fused_computation.11 | convolution fusion | flops 1075314688 | bytes 5767168 | tf_op jit(solution)/shard_map/dot_general | solution.py:160
  249.9 0.0 reduce-scatter.2.cloned.1.call-update
  249.9 7.0 %reduce-scatter.2.cloned.1.call-done = bf16[128,2048]{1,0:T(8,128)(2,1)} async-done(((bf16[256,2048]{1,0:T(8,128)(2,1)}), bf16[128,2048]{1,0:T(8,128)(2,1)}) %reduce-scatter.2.cloned.1.call-update) | async-done | bytes 524304 | tf_op jit(solution)/shard_map/reduce_scatter | solution.py:159
  (36 shorter events, 0.3 us)
Async XLA Ops:
  6.5 4.7 %copy-start = (bf16[256,2048]{1,0:T(8,128)(2,1)S(1)}, bf16[256,2048]{1,0:T(8,128)(2,1)}, u32[]{:S(2)}) copy-start(bf16[256,2048]{1,0:T(8,128)(2,1)} %param.14) | copy-start | bytes 3145732
  6.5 5.0 %copy-start.1 = (bf16[512,128]{1,0:T(8,128)(2,1)S(1)}, bf16[512,128]{1,0:T(8,128)(2,1)}, u32[]{:S(2)}) copy-start(bf16[512,128]{1,0:T(8,128)(2,1)} %param.17) | copy-start | bytes 393220
  6.5 28.1 %copy-start.2 = (bf16[512,128]{1,0:T(8,128)(2,1)S(1)}, bf16[512,128]{1,0:T(8,128)(2,1)}, u32[]{:S(2)}) copy-start(bf16[512,128]{1,0:T(8,128)(2,1)} %param.18) | copy-start | bytes 393220
  6.5 64.6 %all-gather.7.cloned.1.call-start = ((), (), s32[]{:S(2)}) async-start(), calls=%async_computation.2 | async-start | bytes 2621440 | tf_op jit(solution)/shard_map/all_gather | solution.py:86
  7.3 111.1 %all-gather.9.cloned.1.call-start = ((), (), s32[]{:S(2)}) async-start(), calls=%async_computation.3 | async-start | bytes 2621440 | tf_op jit(solution)/shard_map/all_gather | solution.py:87
  8.0 48.4 %copy-start.7 = (f32[2048]{0:T(1024)S(1)}, f32[2048]{0:T(1024)}, u32[]{:S(2)}) copy-start(f32[2048]{0:T(1024)} %param.15) | copy-start | bytes 24580
  8.0 156.6 %all-gather.5.cloned.1.call-start = ((), (), s32[]{:S(2)}) async-start(), calls=%async_computation.1 | async-start | bytes 2621440 | tf_op jit(solution)/shard_map/all_gather | solution.py:83
  8.8 236.7 %all-gather.11.cloned.1.call-start = ((), (), s32[]{:S(2)}) async-start(), calls=%async_computation.4 | async-start | bytes 5242880 | tf_op jit(solution)/shard_map/all_gather | solution.py:158
  11.1 49.1 %copy-start.3 = (f32[31,512]{1,0:T(8,128)S(1)}, f32[31,512]{1,0:T(8,128)}, u32[]{:S(2)}) copy-start(f32[31,512]{1,0:T(8,128)} %param.22) | copy-start | bytes 190468
  11.1 49.5 %copy-start.8 = (f32[8]{0:T(128)S(1)}, f32[8]{0:T(128)}, u32[]{:S(2)}) copy-start(f32[8]{0:T(128)} %param.21) | copy-start | bytes 100
  11.2 245.8 %reduce-scatter.2.cloned.1.call-start = ((), (), s32[]{:S(2)}) async-start(), calls=%async_computation.5 | async-start | bytes 1572864 | tf_op jit(solution)/shard_map/reduce_scatter | solution.py:159
  57.4 4.8 %collective-permute-start = (bf16[128,256]{0,1:T(8,128)(2,1)S(1)}, bf16[128,256]{0,1:T(8,128)(2,1)S(1)}, u32[]{:S(2)}, u32[]{:S(2)}) collective-permute-start(bf16[128,256]{0,1:T(8,128)(2,1)S(1)} %get-tuple-element.21), channel_id=1, source_target_pairs={{0,8},{8,16},{16,24},{1,9},{9,17},{17,25},{2,10},{10,18},{18,26},{... | collective-permute-start | bytes 196616 | tf_op jit(solution)/shard_map/ppermute | solution.py:21
  58.9 10.3 %collective-permute-start.1 = (bf16[128,256]{0,1:T(8,128)(2,1)S(1)}, bf16[128,256]{0,1:T(8,128)(2,1)S(1)}, u32[]{:S(2)}, u32[]{:S(2)}) collective-permute-start(bf16[128,256]{0,1:T(8,128)(2,1)S(1)} %get-tuple-element.22), channel_id=1, source_target_pairs={{8,0},{16,8},{24,16},{9,1},{17,9},{25,17},{10,2},{18,10},{26,18},{... | collective-permute-start | bytes 196616 | tf_op jit(solution)/shard_map/ppermute | solution.py:24
  122.1 48.6 %collective-permute-start.2 = (bf16[15,512]{1,0:T(8,128)(2,1)S(1)}, bf16[15,512]{1,0:T(8,128)(2,1)S(1)}, u32[]{:S(2)}, u32[]{:S(2)}) collective-permute-start(bf16[15,512]{1,0:T(8,128)(2,1)S(1)} %get-tuple-element.15), channel_id=1, source_target_pairs={{0,8},{8,16},{16,24},{1,9},{9,17},{17,25},{2,10},{10,18},{18,26},{... | collective-permute-start | bytes 46088 | tf_op jit(solution)/shard_map/ppermute | solution.py:21
  124.2 46.5 %collective-permute-start.3 = (bf16[15,512]{1,0:T(8,128)(2,1)S(1)}, bf16[15,512]{1,0:T(8,128)(2,1)S(1)}, u32[]{:S(2)}, u32[]{:S(2)}) collective-permute-start(bf16[15,512]{1,0:T(8,128)(2,1)S(1)} %get-tuple-element.16), channel_id=1, source_target_pairs={{8,0},{16,8},{24,16},{9,1},{17,9},{25,17},{10,2},{18,10},{26,18},{... | collective-permute-start | bytes 46088 | tf_op jit(solution)/shard_map/ppermute | solution.py:24
  169.2 1.4 copy-start.4
  169.2 9.7 %copy-start.5 = (f32[512]{0:T(512)S(1)}, f32[512]{0:T(512)}, u32[]{:S(2)}) copy-start(f32[512]{0:T(512)} %param.25) | copy-start | bytes 6148
  169.2 9.7 %copy-start.6 = (f32[512]{0:T(512)S(1)}, f32[512]{0:T(512)}, u32[]{:S(2)}) copy-start(f32[512]{0:T(512)} %param.24) | copy-start | bytes 6148
Sparse Core Ops, SparseCore 0:
  8.9 62.1 all-gather.6
  72.7 45.6 all-gather.8
  120.0 44.6 all-gather.4
  166.1 79.3 all-gather.10
  250.1 6.8 reduce-scatter.1
where the time goes:
time: 264 us
  waiting for transfers between devices  172 us (65%)
  blocking collectives  49.7 us (19%)
  between operations  13.5 us (5%)
  matrix products  13.3 us (5%)
  other arithmetic  6.78 us (3%)
  starting transfers between devices  6.35 us (2%)
    all_gather x1, waiting for transfers between devices, local(): own_whole = lax.all_gather(own_rows, 'sp', axis=1, tiled=True)  66.3 us
    all_gather x1, waiting for transfers between devices, local(): piece_gate = lax.all_gather(w_conv_gate, 'sp', axis=0, tiled=True)  47.3 us
    all_gather x1, waiting for transfers between devices, local(): piece_query = lax.all_gather(w_query, 'sp', axis=0, tiled=True)  39.2 us
    all_gather x1, blocking collectives, local(): piece_key = lax.all_gather(w_key, 'sp', axis=0, tiled=True)  23.1 us
    all_gather x1, blocking collectives, local(): piece_value = lax.all_gather(w_value, 'sp', axis=0, tiled=True)  21.7 us
    reduce_scatter x1, waiting for transfers between devices, local(): lax.psum_scatter(jnp.dot(features, own_whole, preferred_element_type=jnp....  7.04 us
    ppermute x2, waiting for transfers between devices, padded(): lax.ppermute(lax.slice_in_dim(block, 0, width, axis=dim), axis, backward)  6.99 us
  transfers between devices with their start and end apart: 9, of which 7 were waited for; matrix products, arithmetic and copies ran while one was open for 7% of the time, Pallas kernels for 0%

commit v1 on v0

v1 whole, which is shorter than its diff:
```python
import jax
import jax.numpy as jnp
from jax import lax
from jax.sharding import PartitionSpec as P

HEAD_DIM = 64
KV_GROUP = 4
WINDOW = 128
GRID_W = 64


EPSILON = 1e-06
NEGATIVE = -1e30
ROPE_BASE = 10000.0
F32 = jnp.float32
BF16 = jnp.bfloat16


def rotate_pairs(values, positions):
    middle = values.shape[-1] // 2
    inverse = ROPE_BASE ** (-jnp.arange(middle, dtype=F32) / middle)
    angles = positions.astype(F32)[:, None] * inverse[None, :]
    cosine = jnp.cos(angles)[:, None, :]
    sine_table = jnp.sin(angles)[:, None, :]
    leading = values[..., :middle]
    trailing = values[..., middle:]
    return jnp.concatenate(
        [leading * cosine - trailing * sine_table, leading * sine_table + trailing * cosine],
        axis=-1,
    )


def grid_rotate(values, positions):
    middle = values.shape[-1] // 2
    return jnp.concatenate(
        [
            rotate_pairs(values[..., :middle], positions // GRID_W),
            rotate_pairs(values[..., middle:], positions % GRID_W),
        ],
        axis=-1,
    )


def cut(array, start, size, axis):
    return lax.dynamic_slice_in_dim(array, start, size, axis)


def dot(left, right):
    return jnp.dot(left, right, preferred_element_type=F32)


def local(
    tokens,
    norm_gain,
    w_query,
    w_key,
    w_value,
    w_conv_in,
    w_conv_gate,
    sink_logit,
    conv_taps,
    conv_bias,
    channel_gain,
    channel_shift,
    w_attn_out,
    w_conv_out,
):
    sp, fs, tp = (lax.axis_size(a) for a in ("sp", "fs", "tp"))
    s, f, t = (lax.axis_index(a) for a in ("sp", "fs", "tp"))
    width = tokens.shape[1]
    rows = tokens.shape[0] // tp
    depth = width // sp
    head_cols = w_query.shape[1]
    kv_cols = w_key.shape[1]
    heads = head_cols * tp // HEAD_DIM // fs
    q_cols = heads * HEAD_DIM
    kv_here = max(1, heads // KV_GROUP)
    k_cols = kv_here * HEAD_DIM
    group = heads // kv_here
    chan_half = w_conv_in.shape[1] // fs
    chans = chan_half * tp
    reach = conv_taps.shape[0] // 2

    ring = [(i, (i + 1) % sp) for i in range(sp)]
    swap = [(i, tp - 1 - i) for i in range(tp)]
    chain_up = [(i, i + 1) for i in range(sp * tp - 1)]
    chain_down = [(b, a) for a, b in chain_up]

    def onward(x):
        return lax.ppermute(x, "sp", ring)

    def partner(x):
        return lax.ppermute(x, "tp", swap)

    def across(x, step):
        return lax.ppermute(x, "fs", [(i, i ^ step) for i in range(fs)])

    conv_piece = jnp.concatenate(
        [cut(w_conv_in, f * chan_half, chan_half, 1), cut(w_conv_gate, f * chan_half, chan_half, 1)],
        axis=1,
    )
    q_at = f * q_cols
    kv_at = (f * heads // KV_GROUP) * HEAD_DIM
    qkv_piece = jnp.concatenate(
        [
            cut(w_query, q_at % head_cols, q_cols, 1),
            cut(w_key, kv_at % kv_cols, k_cols, 1),
            cut(w_value, kv_at % kv_cols, k_cols, 1),
        ],
        axis=1,
    )
    half = depth // tp
    qkv_other = partner(cut(qkv_piece, (1 - t) * half, half, 0))
    qkv_piece = jnp.where(q_at // head_cols == t, cut(qkv_piece, t * half, half, 0), qkv_other)

    token_float = cut(tokens, t * rows, rows, 0).astype(F32)
    scale = lax.rsqrt(jnp.mean(token_float * token_float, axis=-1, keepdims=True) + EPSILON)
    normed = (token_float * scale * norm_gain[None, :]).astype(BF16)
    normed = jnp.concatenate([cut(normed, ((s - k) % sp) * depth, depth, 1) for k in range(sp)], axis=1)
    gathered = jnp.concatenate([normed] + [across(normed, j) for j in range(1, fs)], axis=0)
    total_rows = fs * rows

    conv_acc = jnp.zeros((total_rows, 4 * chan_half), F32)
    qkv_acc = jnp.zeros((total_rows, q_cols + 2 * k_cols), F32)
    for k in range(sp):
        block = gathered[:, k * depth : (k + 1) * depth]
        conv_other = partner(conv_piece)
        qkv_other = partner(qkv_piece)
        conv_acc = conv_acc + dot(block, jnp.concatenate([conv_piece, conv_other], axis=1))
        mine = cut(block, t * half, half, 1)
        other = cut(block, (1 - t) * half, half, 1)
        qkv_acc = qkv_acc + dot(mine, qkv_piece) + dot(other, qkv_other)
        if k + 1 < sp:
            conv_piece = onward(conv_piece)
            qkv_piece = onward(qkv_piece)

    attn_half = q_cols // tp
    out_piece = jnp.concatenate(
        [
            cut(w_attn_out, q_at + t * attn_half, attn_half, 0),
            cut(w_conv_out, t * w_conv_in.shape[1] + f * chan_half, chan_half, 0),
        ],
        axis=0,
    )
    out_blocks = []
    for k in range(sp):
        out_blocks.append(jnp.concatenate([out_piece, partner(out_piece)], axis=0))
        if k + 1 < sp:
            out_piece = onward(out_piece)

    c2 = 2 * chan_half
    signal = jnp.concatenate([conv_acc[:, :chan_half], conv_acc[:, c2 : c2 + chan_half]], axis=1)
    gate = jnp.concatenate([conv_acc[:, chan_half:c2], conv_acc[:, c2 + chan_half :]], axis=1)
    glu = (signal * jax.nn.sigmoid(gate)).astype(BF16).reshape(fs, rows, chans)

    def chain(x, pairs):
        return lax.ppermute(x, ("sp", "tp"), pairs)

    def other_order(x):
        return jnp.concatenate([x[..., chan_half:], x[..., :chan_half]], axis=-1)

    low = other_order(chain(glu[:, rows - reach :], chain_up))
    high = other_order(chain(glu[:, :reach], chain_down))
    rims = jnp.concatenate([low, glu, high], axis=1).astype(F32)

    def channel(x):
        both = [cut(x, f * chan_half, chan_half, -1)]
        return jnp.concatenate(both + [partner(both[0])], axis=-1)

    vectors = channel(
        jnp.concatenate(
            [conv_taps, conv_bias[None], channel_gain[None], channel_shift[None]], axis=0
        )
    )
    taps = vectors[: 2 * reach + 1]
    bias, gain, shift = (vectors[2 * reach + 1 + i] for i in range(3))
    filtered = jnp.zeros((fs, rows, chans), F32) + bias
    for k in range(2 * reach + 1):
        filtered = filtered + taps[k] * rims[:, k : k + rows]
    own_mean = jnp.sum(filtered, axis=-1) / chans
    own_square = jnp.sum((filtered - own_mean[..., None]) ** 2, axis=-1)
    stats = jnp.stack([own_mean, own_square])
    everyone = [stats]
    for j in range(1, fs):
        there = across(stats, j)
        everyone.append(jnp.stack([there[:, i ^ j] for i in range(fs)], axis=1))
    everyone = jnp.stack(everyone)
    centre = jnp.mean(everyone[:, 0], axis=0)
    spread = (
        jnp.sum(everyone[:, 1], axis=0) + chans * jnp.sum((everyone[:, 0] - centre) ** 2, axis=0)
    ) / (chans * fs)
    conv_out = jax.nn.silu(
        (filtered - centre[..., None]) * lax.rsqrt(spread + EPSILON)[..., None] * gain + shift
    ).astype(BF16).reshape(total_rows, chans)

    start = (s * tp + t) * rows
    positions = start + jnp.arange(rows, dtype=jnp.int32)
    positions_all = jnp.tile(positions, fs)
    query = grid_rotate(qkv_acc[:, :q_cols].reshape(total_rows, heads, HEAD_DIM), positions_all)
    query = query.astype(BF16).reshape(fs, rows, kv_here, group, HEAD_DIM)
    keys = grid_rotate(
        qkv_acc[:, q_cols : q_cols + k_cols].reshape(total_rows, kv_here, HEAD_DIM), positions_all
    ).astype(BF16).reshape(total_rows, k_cols)
    values = qkv_acc[:, q_cols + k_cols :].astype(BF16)
    stacked = jnp.concatenate([keys, values], axis=1).reshape(fs, rows, 2 * k_cols)
    below = chain(stacked[:, rows - WINDOW :], chain_up)
    above = chain(stacked[:, :WINDOW], chain_down)
    extended = jnp.concatenate([below, stacked, above], axis=1)
    span = rows + 2 * WINDOW
    near_keys = extended[..., :k_cols].reshape(fs, span, kv_here, HEAD_DIM)
    near_values = extended[..., k_cols:].reshape(fs, span, kv_here, HEAD_DIM)
    sink_mine = cut(sink_logit, (f * heads) % sink_logit.shape[0], heads, 0)
    sinks = jnp.where(q_at // head_cols == t, sink_mine, partner(sink_mine))
    sinks = sinks.reshape(kv_here, group)[None, :, :, None, None]
    scores = jnp.einsum(
        "fqkgd,fskd->fkgqs", query, near_keys, preferred_element_type=F32
    ) * HEAD_DIM ** (-0.5)
    key_pos = start - WINDOW + jnp.arange(span, dtype=jnp.int32)
    valid = (
        (jnp.abs(positions[:, None] - key_pos[None, :]) <= WINDOW)
        & (key_pos[None, :] >= 0)
        & (key_pos[None, :] < rows * sp * tp)
    )
    scores = jnp.where(valid, scores, NEGATIVE)
    top = jnp.maximum(jnp.max(scores, axis=-1, keepdims=True), sinks)
    raised = jnp.exp(scores - top)
    denominator = jnp.sum(raised, axis=-1, keepdims=True) + jnp.exp(sinks - top)
    probs = (raised / denominator).astype(BF16)
    mixed = jnp.einsum("fkgqs,fskd->fqkgd", probs, near_values, preferred_element_type=F32)
    attended = mixed.astype(BF16).reshape(total_rows, q_cols)

    features = jnp.concatenate(
        [
            cut(attended, t * attn_half, attn_half, 1),
            conv_out[:, :chan_half],
            cut(attended, (1 - t) * attn_half, attn_half, 1),
            conv_out[:, chan_half:],
        ],
        axis=1,
    )
    partial = jnp.concatenate([dot(features, w) for w in out_blocks], axis=1)
    partial = partial.reshape(fs, rows, width)
    result = partial[0]
    for j in range(1, fs):
        result = result + across(partial[j].astype(BF16), j).astype(F32)
    result = result.astype(BF16)
    return jnp.concatenate([cut(result, ((s - k) % sp) * depth, depth, 1) for k in range(sp)], axis=1)


def solution(mesh):
    in_specs = (
        P(("fs", "sp"), None),
        P(),
        P("sp", "tp"),
        P("sp", "tp"),
        P("sp", "tp"),
        P("sp", "tp"),
        P("sp", "tp"),
        P("tp"),
        P(None, "tp"),
        P("tp"),
        P("tp"),
        P("tp"),
        P(None, "sp"),
        P(None, "sp"),
    )
    out_specs = P(("fs", "sp", "tp"), None)
    return jax.shard_map(local, mesh=mesh, in_specs=in_specs, out_specs=out_specs, check_vma=False)
```

time: 264 us -> 163 us (0.62)
  waiting for transfers between devices: 172 us -> 77.8 us
  blocking collectives: 49.7 us -> 0 us
  starting transfers between devices: 6.35 us -> 30.5 us
  other arithmetic: 6.78 us -> 20.9 us
  local copies, waits for them, and re-layouts: 1.64 us -> 15.3 us
  between operations: 13.5 us -> 1.59 us
    all_gather x4 -> x0, waiting for transfers between devices: 155 us -> none  [the longest x1 66.3 us: local(): own_whole = lax.all_gather(own_rows, 'sp', axis=1, tiled=True)]
    ppermute x4 -> x37, waiting for transfers between devices: 8.5 us -> 77.8 us  [the longest x9 38.8 us: across(): return lax.ppermute(x, 'fs', [(i, i ^ step) for i in range(fs)])]
    all_gather x2 -> x0, blocking collectives: 44.8 us -> none  [the longest x1 23.1 us: local(): piece_key = lax.all_gather(w_key, 'sp', axis=0, tiled=True)]
    ppermute x4 -> x37, starting transfers between devices: 6.2 us -> 30.5 us  [the longest x9 11.3 us: across(): return lax.ppermute(x, 'fs', [(i, i ^ step) for i in range(fs)])]
    concatenate x4 -> x10, other arithmetic: 1.1 us -> 8.63 us  [the longest x1 4.1 us: local(): jnp.concatenate([normed] + [across(normed, j) for j in range(1, fs)], axi...]
    reduce_scatter x1 -> x0, waiting for transfers between devices: 7.04 us -> none  [local(): lax.psum_scatter(jnp.dot(features, own_whole, preferred_element_type=jnp....]
    concatenate x0 -> x10, local copies, waits for them, and re-layouts: none -> 6.3 us  [the longest x8 4.65 us: grid_rotate(): jnp.concatenate([rotate_pairs(values[..., :middle], positions // GRID_W),...]
    unnamed x18 -> x121, local copies, waits for them, and re-layouts: 0.04 us -> 5.82 us
  transfers between devices with their start and end apart: 9 -> 37, of which waited for: 7 -> 17; matrix products, arithmetic and copies ran while one was open for 7% -> 27% of each run, Pallas kernels for 0% -> 0%
where the time goes in v1:
time: 163 us; the launch traced here: 160 us
  waiting for transfers between devices  77.8 us (48%)
  starting transfers between devices  30.5 us (19%)
  other arithmetic  20.9 us (13%)
  local copies, waits for them, and re-layouts  15.3 us (9%)
  matrix products  14.1 us (9%)
    ppermute x9, waiting for transfers between devices, across(): return lax.ppermute(x, 'fs', [(i, i ^ step) for i in range(fs)])  38.8 us
    ppermute x9, waiting for transfers between devices, onward(): return lax.ppermute(x, 'sp', ring)  35.8 us
    dot_general x16, matrix products, dot(): return jnp.dot(left, right, preferred_element_type=F32)  12.5 us
    ppermute x9, starting transfers between devices, across(): return lax.ppermute(x, 'fs', [(i, i ^ step) for i in range(fs)])  11.3 us
    ppermute x9, starting transfers between devices, onward(): return lax.ppermute(x, 'sp', ring)  9.35 us
    ppermute x4, starting transfers between devices, chain(): return lax.ppermute(x, ('sp', 'tp'), pairs)  6.9 us
    unnamed x121, local copies, waits for them, and re-layouts  5.82 us
    concatenate x8, local copies, waits for them, and re-layouts, grid_rotate(): jnp.concatenate([rotate_pairs(values[..., :middle], positions // GRID_W),...  4.65 us
  transfers between devices with their start and end apart: 37, of which 17 were waited for; matrix products, arithmetic and copies ran while one was open for 27% of the time, Pallas kernels for 0%

profile of v1, /device:TPU:0, one launch (start us, length us, event | category | flops | bytes accessed | tf_op | source)
XLA Modules:
  0.0 160.2 jit_solution(15981077709470191765)
XLA Ops:
  0.1 1.3 fusion.13
  1.4 1.3 fusion.15
  2.8 3.1 %collective-permute-start = (bf16[128,2048]{1,0:T(8,128)(2,1)S(1)}, bf16[128,2048]{1,0:T(8,128)(2,1)S(1)}, u32[]{:S(2)}, u32[]{:S(2)}) collective-permute-start(bf16[128,2048]{1,0:T(8,128)(2,1)S(1)} %pad_maximum_fusion.2), channel_id=1, source_target_pairs={{0,2},{2,0},{4,6},{6,4},{1,3},{3,1},{5,7},{7,5},{8,10},{10,8},{12,... | collective-permute-start | bytes 1572872 | tf_op jit(solution)/shard_map/ppermute | solution.py:96
  5.9 1.5 collective-permute-start.1
  8.5 1.0 constant_dynamic-slice_fusion.7
  10.2 1.0 constant_dynamic-slice_fusion.4
  18.5 2.1 %collective-permute-start.16 = (bf16[512,256]{1,0:T(8,128)(2,1)}, bf16[512,256]{1,0:T(8,128)(2,1)S(1)}, u32[]{:S(2)}, u32[]{:S(2)}) collective-permute-start(bf16[512,256]{1,0:T(8,128)(2,1)} %pad_maximum_fusion.7), channel_id=1, source_target_pairs={{0,8},{8,16},{16,24},{24,0},{1,9},{9,17},{17,25},{25,1},{2,10},{10... | collective-permute-start | bytes 786440 | tf_op jit(solution)/shard_map/ppermute | solution.py:90
  20.8 9.8 %collective-permute-done.1 = bf16[128,2048]{1,0:T(8,128)(2,1)} collective-permute-done((bf16[128,2048]{1,0:T(8,128)(2,1)S(1)}, bf16[128,2048]{1,0:T(8,128)(2,1)}, u32[]{:S(2)}, u32[]{:S(2)}) %collective-permute-start.1) | collective-permute-done | bytes 524320 | tf_op jit(solution)/shard_map/ppermute | solution.py:96
  30.6 1.6 collective-permute-start.28
  32.2 4.1 %pad_maximum_fusion.1 = bf16[512,2048]{1,0:T(8,128)(2,1)S(1)} fusion(bf16[128,2048]{1,0:T(8,128)(2,1)} %collective-permute-done.2, bf16[128,2048]{1,0:T(8,128)(2,1)} %collective-permute-done.1, bf16[128,2048]{1,0:T(8,128)(2,1)} %copy-done.4, bf16[128,512]{1,0:T(8,128)(2,1)S(1)} %get-tuple-element.31, bf16[128,512]{1,0:T(8,128)(2,1)S(1)} %get-tuple-element.32, ...), kind=kLoop, calls=%fused_computation.6 | loop fusion | flops 14680064 | bytes 4194304 | tf_op jit(solution)/shard_map/concatenate | solution.py:120
  36.5 1.6 %collective-permute-start.5 = (bf16[256,384]{1,0:T(8,128)(2,1)S(1)}, bf16[256,384]{1,0:T(8,128)(2,1)S(1)}, u32[]{:S(2)}, u32[]{:S(2)}) collective-permute-start(bf16[256,384]{1,0:T(8,128)(2,1)S(1)} %dynamic-slice_select_fusion), channel_id=1, source_target_pairs={{0,8},{8,16},{16,24},{24,0},{1,9},{9,17},{17,25},{25,1},{2,10},{10... | collective-permute-start | bytes 589832 | tf_op jit(solution)/shard_map/ppermute | solution.py:90
  39.1 1.3 collective-permute-start.18
  40.3 5.8 %collective-permute-done.5 = bf16[256,384]{1,0:T(8,128)(2,1)S(1)} collective-permute-done((bf16[256,384]{1,0:T(8,128)(2,1)S(1)}, bf16[256,384]{1,0:T(8,128)(2,1)S(1)}, u32[]{:S(2)}, u32[]{:S(2)}) %collective-permute-start.5) | collective-permute-done | bytes 196640 | tf_op jit(solution)/shard_map/ppermute | solution.py:90
  47.0 1.4 collective-permute-start.7
  49.2 2.1 %collective-permute-done.18 = bf16[512,256]{1,0:T(8,128)(2,1)S(1)} collective-permute-done((bf16[512,256]{1,0:T(8,128)(2,1)S(1)}, bf16[512,256]{1,0:T(8,128)(2,1)S(1)}, u32[]{:S(2)}, u32[]{:S(2)}) %collective-permute-start.18) | collective-permute-done | bytes 262176 | tf_op jit(solution)/shard_map/ppermute | solution.py:90
  51.3 10.2 %collective-permute-done.7 = bf16[256,384]{1,0:T(8,128)(2,1)S(1)} collective-permute-done((bf16[256,384]{1,0:T(8,128)(2,1)S(1)}, bf16[256,384]{1,0:T(8,128)(2,1)S(1)}, u32[]{:S(2)}, u32[]{:S(2)}) %collective-permute-start.7) | collective-permute-done | bytes 196640 | tf_op jit(solution)/shard_map/ppermute | solution.py:90
  63.5 1.4 convolution_add_fusion.1
  65.0 8.0 %collective-permute-done.20 = bf16[512,256]{1,0:T(8,128)(2,1)} collective-permute-done((bf16[512,256]{1,0:T(8,128)(2,1)S(1)}, bf16[512,256]{1,0:T(8,128)(2,1)}, u32[]{:S(2)}, u32[]{:S(2)}) %collective-permute-start.20) | collective-permute-done | bytes 262176 | tf_op jit(solution)/shard_map/ppermute | solution.py:90
  73.0 9.3 %collective-permute-done.9 = bf16[256,384]{1,0:T(8,128)(2,1)S(1)} collective-permute-done((bf16[256,384]{1,0:T(8,128)(2,1)S(1)}, bf16[256,384]{1,0:T(8,128)(2,1)S(1)}, u32[]{:S(2)}, u32[]{:S(2)}) %collective-permute-start.9) | collective-permute-done | bytes 196640 | tf_op jit(solution)/shard_map/ppermute | solution.py:90
  85.6 1.3 concatenate.122
  86.9 1.3 copy_dynamic-update-slice_fusion.3
  88.2 1.3 concatenate.123
  89.5 1.3 concatenate.124
  90.9 1.3 copy_dynamic-update-slice_fusion.2
  92.2 1.3 copy_dynamic-update-slice_fusion.1
  94.1 1.3 copy_dynamic-update-slice_fusion
  95.5 1.8 %convolution_add_fusion = f32[512,512]{1,0:T(8,128)S(1)} fusion(f32[512,512]{1,0:T(8,128)} %convolution_add_fusion.1, bf16[512,256]{1,0:T(8,128)(2,1)} %collective-permute-done.21, bf16[512,256]{1,0:T(8,128)(2,1)} %collective-permute-done.20, bf16[512,2048]{1,0:T(8,128)(2,1)S(1)} %pad_maximum_fusion.1), kind=kOutput, calls=%fused_computation.9 | convolution fusion | flops 269746176 | bytes 3145728 | tf_op jit(solution)/shard_map/dot_general | solution.py:49
  97.9 2.2 %collective-permute-start.22 = (bf16[4,15,256]{2,1,0:T(8,128)(2,1)S(1)}, bf16[4,15,256]{2,1,0:T(8,128)(2,1)S(1)}, u32[]{:S(2)}, u32[]{:S(2)}) collective-permute-start(bf16[4,15,256]{2,1,0:T(8,128)(2,1)S(1)} %get-tuple-element.38), channel_id=1, source_target_pairs={{0,1},{1,8},{8,9},{9,16},{16,17},{17,24},{24,25},{2,3},{3,10},{10,... | collective-permute-start | bytes 92168 | tf_op jit(solution)/shard_map/ppermute | solution.py:157
  100.8 1.9 %collective-permute-start.11 = (bf16[4,128,128]{1,2,0:T(8,128)(2,1)}, bf16[4,128,128]{1,2,0:T(8,128)(2,1)S(1)}, u32[]{:S(2)}, u32[]{:S(2)}) collective-permute-start(bf16[4,128,128]{1,2,0:T(8,128)(2,1)} %bitcast_dynamic-update-slice_fusion), channel_id=1, source_target_pairs={{0,1},{1,8},{8,9},{9,16},{16,17},{17,24},{24,25},{2,3},{3,10},{10,... | collective-permute-start | bytes 393224 | tf_op jit(solution)/shard_map/ppermute | solution.py:157
  102.7 1.5 collective-permute-start.23
  104.2 1.6 %collective-permute-done.23 = bf16[4,15,256]{2,1,0:T(8,128)(2,1)S(1)} collective-permute-done((bf16[4,15,256]{2,1,0:T(8,128)(2,1)S(1)}, bf16[4,15,256]{2,1,0:T(8,128)(2,1)S(1)}, u32[]{:S(2)}, u32[]{:S(2)}) %collective-permute-start.23) | collective-permute-done | bytes 30752 | tf_op jit(solution)/shard_map/ppermute | solution.py:157
  106.3 2.3 %fusion.170 = (f32[4,128]{1,0:T(4,128)S(1)}, f32[4,128,256]{2,1,0:T(8,128)S(1)}) fusion(f32[4,158,256]{2,1,0:T(8,128)S(1)} %maximum_convert_fusion, f32[256]{0:T(256)S(1)} %bitcast.228, f32[256]{0:T(256)S(1)} %bitcast.229, f32[256]{0:T(256)S(1)} %bitcast.230, f32[256]{0:T(256)S(1)} %bitcast.231, f32[256]{0:T(256)S(1)} %bitcast.232, f32[256]{0:T(256)S(1)} %bitcast.233, ...), kind=kLoop, calls=%fused_computation.334 | loop fusion | flops 8257024 | bytes 16812032 | tf_op jit(solution)/shard_map/reduce_sum | solution.py:180
  108.8 1.6 collective-permute-start.25
  110.6 1.9 %collective-permute-done.25 = f32[2,4,128]{2,1,0:T(4,128)S(1)} collective-permute-done((f32[2,4,128]{2,1,0:T(4,128)S(1)}, f32[2,4,128]{2,1,0:T(4,128)S(1)}, u32[]{:S(2)}, u32[]{:S(2)}) %collective-permute-start.25) | collective-permute-done | bytes 4128 | tf_op jit(solution)/shard_map/ppermute | solution.py:96
  112.6 3.6 %collective-permute-done.24 = f32[2,4,128]{2,1,0:T(4,128)S(1)} collective-permute-done((f32[2,4,128]{2,1,0:T(4,128)S(1)}, f32[2,4,128]{2,1,0:T(4,128)S(1)}, u32[]{:S(2)}, u32[]{:S(2)}) %collective-permute-start.24) | collective-permute-done | bytes 4128 | tf_op jit(solution)/shard_map/ppermute | solution.py:96
  116.1 1.5 collective-permute-start.26
  117.6 3.0 %collective-permute-done.26 = f32[2,4,128]{2,1,0:T(4,128)S(1)} collective-permute-done((f32[2,4,128]{2,1,0:T(4,128)S(1)}, f32[2,4,128]{2,1,0:T(4,128)S(1)}, u32[]{:S(2)}, u32[]{:S(2)}) %collective-permute-start.26) | collective-permute-done | bytes 4128 | tf_op jit(solution)/shard_map/ppermute | solution.py:96
  120.6 1.3 collective-permute-start.12
  122.6 1.2 collective-permute-start.31
  127.8 1.4 fusion.69
  129.2 1.5 fusion.75
  130.8 1.4 fusion.79
  132.2 1.4 fusion.83
  134.3 2.0 %collective-permute-start.35 = (bf16[128,2048]{0,1:T(8,128)(2,1)S(1)}, bf16[128,2048]{0,1:T(8,128)(2,1)S(1)}, u32[]{:S(2)}, u32[]{:S(2)}) collective-permute-start(bf16[128,2048]{0,1:T(8,128)(2,1)S(1)} %get-tuple-element.11), channel_id=1, source_target_pairs={{0,4},{2,6},{4,0},{6,2},{1,5},{3,7},{5,1},{7,3},{8,12},{10,14},{12... | collective-permute-start | bytes 1572872 | tf_op jit(solution)/shard_map/ppermute | solution.py:96
  136.3 1.4 collective-permute-start.36
  138.2 8.4 %collective-permute-done.34 = bf16[128,2048]{0,1:T(8,128)(2,1)S(1)} collective-permute-done((bf16[128,2048]{0,1:T(8,128)(2,1)S(1)}, bf16[128,2048]{0,1:T(8,128)(2,1)S(1)}, u32[]{:S(2)}, u32[]{:S(2)}) %collective-permute-start.34) | collective-permute-done | bytes 524320 | tf_op jit(solution)/shard_map/ppermute | solution.py:96
  146.8 12.0 %collective-permute-done.36 = bf16[128,2048]{0,1:T(8,128)(2,1)S(1)} collective-permute-done((bf16[128,2048]{0,1:T(8,128)(2,1)S(1)}, bf16[128,2048]{0,1:T(8,128)(2,1)S(1)}, u32[]{:S(2)}, u32[]{:S(2)}) %collective-permute-start.36) | collective-permute-done | bytes 524320 | tf_op jit(solution)/shard_map/ppermute | solution.py:96
  159.1 1.0 copy.34
  (245 shorter events, 25.6 us)
Async XLA Ops:
  2.7 11.1 %copy-start.53 = (f32[512]{0:T(512)S(1)}, f32[512]{0:T(512)}, u32[]{:S(2)}) copy-start(f32[512]{0:T(512)} %param.23) | copy-start | bytes 6148
  2.7 11.1 %copy-start.54 = (f32[512]{0:T(512)S(1)}, f32[512]{0:T(512)}, u32[]{:S(2)}) copy-start(f32[512]{0:T(512)} %param.24) | copy-start | bytes 6148
  2.7 11.1 %copy-start.55 = (f32[512]{0:T(512)S(1)}, f32[512]{0:T(512)}, u32[]{:S(2)}) copy-start(f32[512]{0:T(512)} %param.25) | copy-start | bytes 6148
  2.8 17.8 %collective-permute-start = (bf16[128,2048]{1,0:T(8,128)(2,1)S(1)}, bf16[128,2048]{1,0:T(8,128)(2,1)S(1)}, u32[]{:S(2)}, u32[]{:S(2)}) collective-permute-start(bf16[128,2048]{1,0:T(8,128)(2,1)S(1)} %pad_maximum_fusion.2), channel_id=1, source_target_pairs={{0,2},{2,0},{4,6},{6,4},{1,3},{3,1},{5,7},{7,5},{8,10},{10,8},{12,... | collective-permute-start | bytes 1572872 | tf_op jit(solution)/shard_map/ppermute | solution.py:96
  5.9 24.7 %collective-permute-start.1 = (bf16[128,2048]{1,0:T(8,128)(2,1)S(1)}, bf16[128,2048]{1,0:T(8,128)(2,1)}, u32[]{:S(2)}, u32[]{:S(2)}) collective-permute-start(bf16[128,2048]{1,0:T(8,128)(2,1)S(1)} %pad_maximum_fusion.2), channel_id=1, source_target_pairs={{0,4},{2,6},{4,0},{6,2},{1,5},{3,7},{5,1},{7,3},{8,12},{10,14},{12... | collective-permute-start | bytes 1572872 | tf_op jit(solution)/shard_map/ppermute | solution.py:96
  7.4 24.8 %collective-permute-start.2 = (bf16[128,2048]{1,0:T(8,128)(2,1)S(1)}, bf16[128,2048]{1,0:T(8,128)(2,1)}, u32[]{:S(2)}, u32[]{:S(2)}) collective-permute-start(bf16[128,2048]{1,0:T(8,128)(2,1)S(1)} %pad_maximum_fusion.2), channel_id=1, source_target_pairs={{0,6},{2,4},{4,2},{6,0},{1,7},{3,5},{5,3},{7,1},{8,14},{10,12},{12... | collective-permute-start | bytes 1572872 | tf_op jit(solution)/shard_map/ppermute | solution.py:96
  7.7 10.7 %collective-permute-start.3 = (bf16[256,384]{1,0:T(8,128)(2,1)S(1)}, bf16[256,384]{1,0:T(8,128)(2,1)S(1)}, u32[]{:S(2)}, u32[]{:S(2)}) collective-permute-start(bf16[256,384]{1,0:T(8,128)(2,1)S(1)} %constant_dynamic-slice_fusion.10), channel_id=1, source_target_pairs={{0,1},{1,0},{2,3},{3,2},{4,5},{5,4},{6,7},{7,6},{8,9},{9,8},{10,11... | collective-permute-start | bytes 589832 | tf_op jit(solution)/shard_map/ppermute | solution.py:93
  7.9 6.7 %collective-permute-start.13 = (f32[4]{0:T(128)S(1)}, f32[4]{0:T(128)S(1)}, u32[]{:S(2)}, u32[]{:S(2)}) collective-permute-start(f32[4]{0:T(128)S(1)} %dynamic_slice.108), channel_id=1, source_target_pairs={{0,1},{1,0},{2,3},{3,2},{4,5},{5,4},{6,7},{7,6},{8,9},{9,8},{10,11... | collective-permute-start | bytes 56 | tf_op jit(solution)/shard_map/ppermute | solution.py:93
  11.2 20.9 %copy-start.2 = (bf16[128,512]{1,0:T(8,128)(2,1)}, bf16[128,512]{1,0:T(8,128)(2,1)S(1)}, u32[]{:S(2)}) copy-start(bf16[128,512]{1,0:T(8,128)(2,1)S(1)} %get-tuple-element.109) | copy-start | bytes 393220
  14.6 1.2 collective-permute-start.14
  15.8 30.7 %collective-permute-start.15 = (bf16[512,256]{1,0:T(8,128)(2,1)}, bf16[512,256]{1,0:T(8,128)(2,1)S(1)}, u32[]{:S(2)}, u32[]{:S(2)}) collective-permute-start(bf16[512,256]{1,0:T(8,128)(2,1)} %pad_maximum_fusion.7), channel_id=1, source_target_pairs={{0,1},{1,0},{2,3},{3,2},{4,5},{5,4},{6,7},{7,6},{8,9},{9,8},{10,11... | collective-permute-start | bytes 786440 | tf_op jit(solution)/shard_map/ppermute | solution.py:93
  18.5 18.0 %collective-permute-start.16 = (bf16[512,256]{1,0:T(8,128)(2,1)}, bf16[512,256]{1,0:T(8,128)(2,1)S(1)}, u32[]{:S(2)}, u32[]{:S(2)}) collective-permute-start(bf16[512,256]{1,0:T(8,128)(2,1)} %pad_maximum_fusion.7), channel_id=1, source_target_pairs={{0,8},{8,16},{16,24},{24,0},{1,9},{9,17},{17,25},{25,1},{2,10},{10... | collective-permute-start | bytes 786440 | tf_op jit(solution)/shard_map/ppermute | solution.py:90
  20.6 11.5 %copy-start.4 = (bf16[128,2048]{1,0:T(8,128)(2,1)}, bf16[128,2048]{1,0:T(8,128)(2,1)S(1)}, u32[]{:S(2)}) copy-start(bf16[128,2048]{1,0:T(8,128)(2,1)S(1)} %collective-permute-done) | copy-start | bytes 1572868
  20.6 107.1 %collective-permute-start.27 = (bf16[256,512]{1,0:T(8,128)(2,1)}, bf16[256,512]{1,0:T(8,128)(2,1)}, u32[]{:S(2)}, u32[]{:S(2)}) collective-permute-start(bf16[256,512]{1,0:T(8,128)(2,1)} %pad_maximum_fusion.8), channel_id=1, source_target_pairs={{0,1},{1,0},{2,3},{3,2},{4,5},{5,4},{6,7},{7,6},{8,9},{9,8},{10,11... | collective-permute-start | bytes 786440 | tf_op jit(solution)/shard_map/ppermute | solution.py:93
  30.6 8.5 %collective-permute-start.28 = (bf16[256,512]{1,0:T(8,128)(2,1)}, bf16[256,512]{1,0:T(8,128)(2,1)}, u32[]{:S(2)}, u32[]{:S(2)}) collective-permute-start(bf16[256,512]{1,0:T(8,128)(2,1)} %pad_maximum_fusion.8), channel_id=1, source_target_pairs={{0,8},{8,16},{16,24},{24,0},{1,9},{9,17},{17,25},{25,1},{2,10},{10... | collective-permute-start | bytes 786440 | tf_op jit(solution)/shard_map/ppermute | solution.py:90
  32.2 6.0 %collective-permute-start.4 = (bf16[256,384]{1,0:T(8,128)(2,1)S(1)}, bf16[256,384]{1,0:T(8,128)(2,1)S(1)}, u32[]{:S(2)}, u32[]{:S(2)}) collective-permute-start(bf16[256,384]{1,0:T(8,128)(2,1)S(1)} %dynamic-slice_select_fusion), channel_id=1, source_target_pairs={{0,1},{1,0},{2,3},{3,2},{4,5},{5,4},{6,7},{7,6},{8,9},{9,8},{10,11... | collective-permute-start | bytes 589832 | tf_op jit(solution)/shard_map/ppermute | solution.py:93
  36.5 9.6 %collective-permute-start.5 = (bf16[256,384]{1,0:T(8,128)(2,1)S(1)}, bf16[256,384]{1,0:T(8,128)(2,1)S(1)}, u32[]{:S(2)}, u32[]{:S(2)}) collective-permute-start(bf16[256,384]{1,0:T(8,128)(2,1)S(1)} %dynamic-slice_select_fusion), channel_id=1, source_target_pairs={{0,8},{8,16},{16,24},{24,0},{1,9},{9,17},{17,25},{25,1},{2,10},{10... | collective-permute-start | bytes 589832 | tf_op jit(solution)/shard_map/ppermute | solution.py:90
  38.2 8.8 %collective-permute-start.17 = (bf16[512,256]{1,0:T(8,128)(2,1)S(1)}, bf16[512,256]{1,0:T(8,128)(2,1)S(1)}, u32[]{:S(2)}, u32[]{:S(2)}) collective-permute-start(bf16[512,256]{1,0:T(8,128)(2,1)S(1)} %collective-permute-done.16), channel_id=1, source_target_pairs={{0,1},{1,0},{2,3},{3,2},{4,5},{5,4},{6,7},{7,6},{8,9},{9,8},{10,11... | collective-permute-start | bytes 786440 | tf_op jit(solution)/shard_map/ppermute | solution.py:93
  39.1 12.2 %collective-permute-start.18 = (bf16[512,256]{1,0:T(8,128)(2,1)S(1)}, bf16[512,256]{1,0:T(8,128)(2,1)S(1)}, u32[]{:S(2)}, u32[]{:S(2)}) collective-permute-start(bf16[512,256]{1,0:T(8,128)(2,1)S(1)} %collective-permute-done.16), channel_id=1, source_target_pairs={{0,8},{8,16},{16,24},{24,0},{1,9},{9,17},{17,25},{25,1},{2,10},{10... | collective-permute-start | bytes 786440 | tf_op jit(solution)/shard_map/ppermute | solution.py:90
  46.2 83.1 %collective-permute-start.29 = (bf16[256,512]{1,0:T(8,128)(2,1)}, bf16[256,512]{1,0:T(8,128)(2,1)}, u32[]{:S(2)}, u32[]{:S(2)}) collective-permute-start(bf16[256,512]{1,0:T(8,128)(2,1)} %collective-permute-done.28), channel_id=1, source_target_pairs={{0,1},{1,0},{2,3},{3,2},{4,5},{5,4},{6,7},{7,6},{8,9},{9,8},{10,11... | collective-permute-start | bytes 786440 | tf_op jit(solution)/shard_map/ppermute | solution.py:93
  46.5 15.3 %collective-permute-start.30 = (bf16[256,512]{1,0:T(8,128)(2,1)}, bf16[256,512]{1,0:T(8,128)(2,1)}, u32[]{:S(2)}, u32[]{:S(2)}) collective-permute-start(bf16[256,512]{1,0:T(8,128)(2,1)} %collective-permute-done.28), channel_id=1, source_target_pairs={{0,8},{8,16},{16,24},{24,0},{1,9},{9,17},{17,25},{25,1},{2,10},{10... | collective-permute-start | bytes 786440 | tf_op jit(solution)/shard_map/ppermute | solution.py:90
  47.0 14.5 %collective-permute-start.7 = (bf16[256,384]{1,0:T(8,128)(2,1)S(1)}, bf16[256,384]{1,0:T(8,128)(2,1)S(1)}, u32[]{:S(2)}, u32[]{:S(2)}) collective-permute-start(bf16[256,384]{1,0:T(8,128)(2,1)S(1)} %collective-permute-done.5), channel_id=1, source_target_pairs={{0,8},{8,16},{16,24},{24,0},{1,9},{9,17},{17,25},{25,1},{2,10},{10... | collective-permute-start | bytes 589832 | tf_op jit(solution)/shard_map/ppermute | solution.py:90
  51.3 10.6 %collective-permute-start.6 = (bf16[256,384]{1,0:T(8,128)(2,1)S(1)}, bf16[256,384]{1,0:T(8,128)(2,1)S(1)}, u32[]{:S(2)}, u32[]{:S(2)}) collective-permute-start(bf16[256,384]{1,0:T(8,128)(2,1)S(1)} %collective-permute-done.5), channel_id=1, source_target_pairs={{0,1},{1,0},{2,3},{3,2},{4,5},{5,4},{6,7},{7,6},{8,9},{9,8},{10,11... | collective-permute-start | bytes 589832 | tf_op jit(solution)/shard_map/ppermute | solution.py:93
  61.5 1.7 %collective-permute-start.19 = (bf16[512,256]{1,0:T(8,128)(2,1)S(1)}, bf16[512,256]{1,0:T(8,128)(2,1)S(1)}, u32[]{:S(2)}, u32[]{:S(2)}) collective-permute-start(bf16[512,256]{1,0:T(8,128)(2,1)S(1)} %collective-permute-done.18), channel_id=1, source_target_pairs={{0,1},{1,0},{2,3},{3,2},{4,5},{5,4},{6,7},{7,6},{8,9},{9,8},{10,11... | collective-permute-start | bytes 786440 | tf_op jit(solution)/shard_map/ppermute | solution.py:93
  61.8 11.1 %collective-permute-start.20 = (bf16[512,256]{1,0:T(8,128)(2,1)S(1)}, bf16[512,256]{1,0:T(8,128)(2,1)}, u32[]{:S(2)}, u32[]{:S(2)}) collective-permute-start(bf16[512,256]{1,0:T(8,128)(2,1)S(1)} %collective-permute-done.18), channel_id=1, source_target_pairs={{0,8},{8,16},{16,24},{24,0},{1,9},{9,17},{17,25},{25,1},{2,10},{10... | collective-permute-start | bytes 786440 | tf_op jit(solution)/shard_map/ppermute | solution.py:90
  61.9 60.7 %collective-permute-start.32 = (bf16[256,512]{1,0:T(8,128)(2,1)}, bf16[256,512]{1,0:T(8,128)(2,1)}, u32[]{:S(2)}, u32[]{:S(2)}) collective-permute-start(bf16[256,512]{1,0:T(8,128)(2,1)} %collective-permute-done.30), channel_id=1, source_target_pairs={{0,8},{8,16},{16,24},{24,0},{1,9},{9,17},{17,25},{25,1},{2,10},{10... | collective-permute-start | bytes 786440 | tf_op jit(solution)/shard_map/ppermute | solution.py:90
  63.2 19.0 %collective-permute-start.9 = (bf16[256,384]{1,0:T(8,128)(2,1)S(1)}, bf16[256,384]{1,0:T(8,128)(2,1)S(1)}, u32[]{:S(2)}, u32[]{:S(2)}) collective-permute-start(bf16[256,384]{1,0:T(8,128)(2,1)S(1)} %collective-permute-done.7), channel_id=1, source_target_pairs={{0,8},{8,16},{16,24},{24,0},{1,9},{9,17},{17,25},{25,1},{2,10},{10... | collective-permute-start | bytes 589832 | tf_op jit(solution)/shard_map/ppermute | solution.py:90
  72.9 9.6 %collective-permute-start.8 = (bf16[256,384]{1,0:T(8,128)(2,1)S(1)}, bf16[256,384]{1,0:T(8,128)(2,1)S(1)}, u32[]{:S(2)}, u32[]{:S(2)}) collective-permute-start(bf16[256,384]{1,0:T(8,128)(2,1)S(1)} %collective-permute-done.7), channel_id=1, source_target_pairs={{0,1},{1,0},{2,3},{3,2},{4,5},{5,4},{6,7},{7,6},{8,9},{9,8},{10,11... | collective-permute-start | bytes 589832 | tf_op jit(solution)/shard_map/ppermute | solution.py:93
  82.2 13.2 %collective-permute-start.21 = (bf16[512,256]{1,0:T(8,128)(2,1)}, bf16[512,256]{1,0:T(8,128)(2,1)}, u32[]{:S(2)}, u32[]{:S(2)}) collective-permute-start(bf16[512,256]{1,0:T(8,128)(2,1)} %collective-permute-done.20), channel_id=1, source_target_pairs={{0,1},{1,0},{2,3},{3,2},{4,5},{5,4},{6,7},{7,6},{8,9},{9,8},{10,11... | collective-permute-start | bytes 786440 | tf_op jit(solution)/shard_map/ppermute | solution.py:93
  82.6 1.7 %collective-permute-start.10 = (bf16[256,384]{1,0:T(8,128)(2,1)S(1)}, bf16[256,384]{1,0:T(8,128)(2,1)S(1)}, u32[]{:S(2)}, u32[]{:S(2)}) collective-permute-start(bf16[256,384]{1,0:T(8,128)(2,1)S(1)} %collective-permute-done.9), channel_id=1, source_target_pairs={{0,1},{1,0},{2,3},{3,2},{4,5},{5,4},{6,7},{7,6},{8,9},{9,8},{10,11... | collective-permute-start | bytes 589832 | tf_op jit(solution)/shard_map/ppermute | solution.py:93
  84.6 16.2 %copy-start.1 = (f32[512,384]{0,1:T(8,128)}, f32[512,384]{0,1:T(8,128)S(1)}, u32[]{:S(2)}) copy-start(f32[512,384]{0,1:T(8,128)S(1)} %convolution_add_fusion.3) | copy-start | bytes 2359300
  97.3 8.6 %copy-start.19 = (f32[1,256]{1,0:T(1,128)S(1)}, f32[1,256]{1,0:T(1,128)}, u32[]{:S(2)}) copy-start(f32[1,256]{1,0:T(1,128)} %get-tuple-element.64) | copy-start | bytes 3076
  97.3 8.6 %copy-start.20 = (f32[1,256]{1,0:T(1,128)S(1)}, f32[1,256]{1,0:T(1,128)}, u32[]{:S(2)}) copy-start(f32[1,256]{1,0:T(1,128)} %get-tuple-element.65) | copy-start | bytes 3076
  97.9 4.8 %collective-permute-start.22 = (bf16[4,15,256]{2,1,0:T(8,128)(2,1)S(1)}, bf16[4,15,256]{2,1,0:T(8,128)(2,1)S(1)}, u32[]{:S(2)}, u32[]{:S(2)}) collective-permute-start(bf16[4,15,256]{2,1,0:T(8,128)(2,1)S(1)} %get-tuple-element.38), channel_id=1, source_target_pairs={{0,1},{1,8},{8,9},{9,16},{16,17},{17,24},{24,25},{2,3},{3,10},{10,... | collective-permute-start | bytes 92168 | tf_op jit(solution)/shard_map/ppermute | solution.py:157
  100.8 23.0 %collective-permute-start.11 = (bf16[4,128,128]{1,2,0:T(8,128)(2,1)}, bf16[4,128,128]{1,2,0:T(8,128)(2,1)S(1)}, u32[]{:S(2)}, u32[]{:S(2)}) collective-permute-start(bf16[4,128,128]{1,2,0:T(8,128)(2,1)} %bitcast_dynamic-update-slice_fusion), channel_id=1, source_target_pairs={{0,1},{1,8},{8,9},{9,16},{16,17},{17,24},{24,25},{2,3},{3,10},{10,... | collective-permute-start | bytes 393224 | tf_op jit(solution)/shard_map/ppermute | solution.py:157
  102.7 3.1 %collective-permute-start.23 = (bf16[4,15,256]{2,1,0:T(8,128)(2,1)S(1)}, bf16[4,15,256]{2,1,0:T(8,128)(2,1)S(1)}, u32[]{:S(2)}, u32[]{:S(2)}) collective-permute-start(bf16[4,15,256]{2,1,0:T(8,128)(2,1)S(1)} %get-tuple-element.39), channel_id=1, source_target_pairs={{1,0},{8,1},{9,8},{16,9},{17,16},{24,17},{25,24},{3,2},{10,3},{11,... | collective-permute-start | bytes 92168 | tf_op jit(solution)/shard_map/ppermute | solution.py:157
  106.2 15.8 %copy-start.17 = (f32[1,256]{1,0:T(1,128)S(1)}, f32[1,256]{1,0:T(1,128)}, u32[]{:S(2)}) copy-start(f32[1,256]{1,0:T(1,128)} %get-tuple-element.55) | copy-start | bytes 3076
  106.3 15.8 %copy-start.18 = (f32[1,256]{1,0:T(1,128)S(1)}, f32[1,256]{1,0:T(1,128)}, u32[]{:S(2)}) copy-start(f32[1,256]{1,0:T(1,128)} %get-tuple-element.46) | copy-start | bytes 3076
  108.5 16.5 %copy-start.5 = (pred[128,384]{0,1:T(8,128)(4,1)S(1)}, pred[128,384]{0,1:T(8,128)(4,1)}, u32[]{:S(2)}) copy-start(pred[128,384]{0,1:T(8,128)(4,1)} %fusion.108) | copy-start | bytes 147460
  108.8 3.7 %collective-permute-start.25 = (f32[2,4,128]{2,1,0:T(4,128)S(1)}, f32[2,4,128]{2,1,0:T(4,128)S(1)}, u32[]{:S(2)}, u32[]{:S(2)}) collective-permute-start(f32[2,4,128]{2,1,0:T(4,128)S(1)} %get-tuple-element.85), channel_id=1, source_target_pairs={{0,4},{2,6},{4,0},{6,2},{1,5},{3,7},{5,1},{7,3},{8,12},{10,14},{12... | collective-permute-start | bytes 12296 | tf_op jit(solution)/shard_map/ppermute | solution.py:96
  112.5 3.6 %collective-permute-start.24 = (f32[2,4,128]{2,1,0:T(4,128)S(1)}, f32[2,4,128]{2,1,0:T(4,128)S(1)}, u32[]{:S(2)}, u32[]{:S(2)}) collective-permute-start(f32[2,4,128]{2,1,0:T(4,128)S(1)} %get-tuple-element.85), channel_id=1, source_target_pairs={{0,2},{2,0},{4,6},{6,4},{1,3},{3,1},{5,7},{7,5},{8,10},{10,8},{12,... | collective-permute-start | bytes 12296 | tf_op jit(solution)/shard_map/ppermute | solution.py:96
  116.1 4.5 %collective-permute-start.26 = (f32[2,4,128]{2,1,0:T(4,128)S(1)}, f32[2,4,128]{2,1,0:T(4,128)S(1)}, u32[]{:S(2)}, u32[]{:S(2)}) collective-permute-start(f32[2,4,128]{2,1,0:T(4,128)S(1)} %get-tuple-element.85), channel_id=1, source_target_pairs={{0,6},{2,4},{4,2},{6,0},{1,7},{3,5},{5,3},{7,1},{8,14},{10,12},{12... | collective-permute-start | bytes 12296 | tf_op jit(solution)/shard_map/ppermute | solution.py:96
  120.6 3.4 %collective-permute-start.12 = (bf16[4,128,128]{1,2,0:T(8,128)(2,1)}, bf16[4,128,128]{1,2,0:T(8,128)(2,1)S(1)}, u32[]{:S(2)}, u32[]{:S(2)}) collective-permute-start(bf16[4,128,128]{1,2,0:T(8,128)(2,1)} %bitcast_dynamic-update-slice_fusion), channel_id=1, source_target_pairs={{1,0},{8,1},{9,8},{16,9},{17,16},{24,17},{25,24},{3,2},{10,3},{11,... | collective-permute-start | bytes 393224 | tf_op jit(solution)/shard_map/ppermute | solution.py:157
  122.6 8.1 %collective-permute-start.31 = (bf16[256,512]{1,0:T(8,128)(2,1)}, bf16[256,512]{1,0:T(8,128)(2,1)S(1)}, u32[]{:S(2)}, u32[]{:S(2)}) collective-permute-start(bf16[256,512]{1,0:T(8,128)(2,1)} %collective-permute-done.30), channel_id=1, source_target_pairs={{0,1},{1,0},{2,3},{3,2},{4,5},{5,4},{6,7},{7,6},{8,9},{9,8},{10,11... | collective-permute-start | bytes 786440 | tf_op jit(solution)/shard_map/ppermute | solution.py:93
  123.8 8.4 %collective-permute-start.33 = (bf16[256,512]{1,0:T(8,128)(2,1)}, bf16[256,512]{1,0:T(8,128)(2,1)S(1)}, u32[]{:S(2)}, u32[]{:S(2)}) collective-permute-start(bf16[256,512]{1,0:T(8,128)(2,1)} %collective-permute-done.32), channel_id=1, source_target_pairs={{0,1},{1,0},{2,3},{3,2},{4,5},{5,4},{6,7},{7,6},{8,9},{9,8},{10,11... | collective-permute-start | bytes 786440 | tf_op jit(solution)/shard_map/ppermute | solution.py:93
  134.2 12.4 %collective-permute-start.34 = (bf16[128,2048]{0,1:T(8,128)(2,1)S(1)}, bf16[128,2048]{0,1:T(8,128)(2,1)S(1)}, u32[]{:S(2)}, u32[]{:S(2)}) collective-permute-start(bf16[128,2048]{0,1:T(8,128)(2,1)S(1)} %get-tuple-element.9), channel_id=1, source_target_pairs={{0,2},{2,0},{4,6},{6,4},{1,3},{3,1},{5,7},{7,5},{8,10},{10,8},{12,... | collective-permute-start | bytes 1572872 | tf_op jit(solution)/shard_map/ppermute | solution.py:96
  134.3 12.5 %collective-permute-start.35 = (bf16[128,2048]{0,1:T(8,128)(2,1)S(1)}, bf16[128,2048]{0,1:T(8,128)(2,1)S(1)}, u32[]{:S(2)}, u32[]{:S(2)}) collective-permute-start(bf16[128,2048]{0,1:T(8,128)(2,1)S(1)} %get-tuple-element.11), channel_id=1, source_target_pairs={{0,4},{2,6},{4,0},{6,2},{1,5},{3,7},{5,1},{7,3},{8,12},{10,14},{12... | collective-permute-start | bytes 1572872 | tf_op jit(solution)/shard_map/ppermute | solution.py:96
  136.3 22.5 %collective-permute-start.36 = (bf16[128,2048]{0,1:T(8,128)(2,1)S(1)}, bf16[128,2048]{0,1:T(8,128)(2,1)S(1)}, u32[]{:S(2)}, u32[]{:S(2)}) collective-permute-start(bf16[128,2048]{0,1:T(8,128)(2,1)S(1)} %get-tuple-element.10), channel_id=1, source_target_pairs={{0,6},{2,4},{4,2},{6,0},{1,7},{3,5},{5,3},{7,1},{8,14},{10,12},{12... | collective-permute-start | bytes 1572872 | tf_op jit(solution)/shard_map/ppermute | solution.py:96
  (47 other events, 336.4 us)
